TPU v7x, 32 devices: a whole 2x2x4 slice. The times are simulated.
32 devices in a mesh: sp: 8 (over z, x), tp: 4 (over y, core).
Axes of the slice: x: 2, y: 2, z: 4, core: 2. Of those that a mesh axis runs over, the one named last changes fastest.
Arguments:
- layer_grad: bfloat16 [2048, 2048], P('sp', 'tp'), may hold values from -6 to 6
- routes: int32 [2048, 2], P('sp'), may hold values from 0 to 7, all different within a row; in each aligned block of 256 rows (0 to 255, 256 to 511, ...) at most 96 rows name the same one
- route_weights: float32 [2048, 2], P('sp'), may hold values from 0.1 to 0.9
- expert_in: bfloat16 [8, 768, 2048], P('sp', None, 'tp'), may hold values from -50 to 50
- w_gate: bfloat16 [8, 2048, 2048], P('sp', None, 'tp'), may hold values from -0.125 to 0.125
- w_up: bfloat16 [8, 2048, 2048], P('sp', None, 'tp'), may hold values from -0.125 to 0.125
- w_down: bfloat16 [8, 2048, 2048], P('sp', 'tp'), may hold values from -0.125 to 0.125
- conv_in: bfloat16 [2048, 512], P('sp', 'tp'), may hold values from -6 to 6
- c_gate: bfloat16 [2048, 512], P('sp', 'tp'), may hold values from -6 to 6
- b_gate: bfloat16 [2048, 512], P('sp', 'tp'), may hold values from -1.5 to 1.5
- conv_out: bfloat16 [2048, 512], P('sp', 'tp'), may hold values from -1.5 to 1.5
- taps: bfloat16 [3, 512], P(None, 'tp'), may hold values from -3.5 to 3.5
- w_out: bfloat16 [512, 2048], P('tp'), may hold values from -0.25 to 0.25
Outputs:
- grad_w_gate: bfloat16 [8, 2048, 2048], P('sp', None, 'tp')
- grad_w_up: bfloat16 [8, 2048, 2048], P('sp', None, 'tp')
- grad_w_down: bfloat16 [8, 2048, 2048], P('sp', 'tp')
- grad_routed: bfloat16 [2048, 2048], P('sp', 'tp')
- grad_out_proj: float32 [512, 2048], P('tp', 'sp')
- grad_conv_in: bfloat16 [2048, 512], P('sp', 'tp')
- grad_c_gate: bfloat16 [2048, 512], P('sp', 'tp')
- grad_b_gate: bfloat16 [2048, 512], P('sp', 'tp')
Inputs may be any that keep to these rules, and one draw needn't show every extreme that they name: `routes`: each token names 2 different experts. Among the tokens of one block of 256, no expert is named more than 96 times, a bound that some block reaches.
All inputs are finite; a program needn't handle non-finite values.
Results may differ from a plain program's by a relative error of at most 0.019.
Values may be sent and summed in bfloat16 or wider, within the bound.
No kernel may reach another device: no remote copies, remote signals or barrier semaphores. Data moves between devices by JAX's collectives and lax.ppermute only.
A program may use at most 64 MiB of HBM per device.

v0:
```python
import jax
import jax.numpy as jnp
from jax import lax
from jax.sharding import PartitionSpec as P

clamp_limit = 7.0
swish_alpha = 1.702


def passed_along(value, axis, steps):
    count = lax.axis_size(axis)
    leading, last = (max(0, -steps), min(count, count - steps))
    return lax.ppermute(value, axis, [(source, source + steps) for source in range(leading, last)])


def per_device(
    layer_grad,
    routes,
    route_weights,
    expert_in,
    w_gate,
    w_up,
    w_down,
    conv_in,
    c_gate,
    b_gate,
    conv_out,
    taps,
    w_out,
):
    sp_devices = lax.axis_size("sp")
    tok_rows = layer_grad.shape[0]
    top_count = routes.shape[1]
    capacity = expert_in.shape[1] // sp_devices
    full_grad = lax.all_gather(layer_grad, "tp", axis=1, tiled=True)
    flat_routes = routes.reshape(-1)
    onehot = (flat_routes[:, None] == jnp.arange(sp_devices, dtype=jnp.int32)[None, :]).astype(
        jnp.int32
    )
    slot_rank = jnp.sum((jnp.cumsum(onehot, axis=0) - 1) * onehot, axis=1)
    slot_index = flat_routes * capacity + slot_rank
    weights = route_weights[:, :, None]
    scaled = (weights * layer_grad[:, None, :].astype(jnp.float32)).astype(jnp.bfloat16)
    scaled = scaled.reshape(tok_rows * top_count, -1)
    buffer = (
        jnp.zeros((sp_devices * capacity, scaled.shape[1]), jnp.bfloat16).at[slot_index].set(scaled)
    )
    arrived = lax.all_to_all(
        buffer.reshape(sp_devices, capacity, -1), "sp", split_axis=0, concat_axis=0, tiled=True
    )
    expert_grad, saved_rows = (
        lax.all_gather(arrived.reshape(sp_devices * capacity, -1), "tp", axis=1, tiled=True),
        lax.all_gather(expert_in[0], "tp", axis=1, tiled=True),
    )
    gate_weight = w_gate[0]
    up_weight = w_up[0]
    down_weight = w_down[0]
    gate_pre = jnp.dot(saved_rows, gate_weight, preferred_element_type=jnp.float32)
    up_pre = jnp.dot(saved_rows, up_weight, preferred_element_type=jnp.float32)
    gate_cut = jnp.minimum(gate_pre, clamp_limit)
    up_cut = jnp.clip(up_pre, -clamp_limit, clamp_limit)
    sigmoid_gate = jax.nn.sigmoid(swish_alpha * gate_cut)
    hidden = ((up_cut + 1.0) * gate_cut * sigmoid_gate).astype(jnp.bfloat16)
    act_grad = jnp.einsum("rd,fd->rf", expert_grad, down_weight, preferred_element_type=jnp.float32)
    grad_down = jnp.einsum(
        "rf,rd->fd", hidden, expert_grad, preferred_element_type=jnp.float32
    ).astype(jnp.bfloat16)
    slope = sigmoid_gate + swish_alpha * gate_cut * sigmoid_gate * (1.0 - sigmoid_gate)
    gate_grad = jnp.where(gate_pre < clamp_limit, act_grad * (up_cut + 1.0) * slope, 0.0).astype(
        jnp.bfloat16
    )
    up_grad = jnp.where(
        jnp.abs(up_pre) < clamp_limit, act_grad * gate_cut * sigmoid_gate, 0.0
    ).astype(jnp.bfloat16)
    grad_gate = jnp.einsum(
        "rd,rf->df", saved_rows, gate_grad, preferred_element_type=jnp.float32
    ).astype(jnp.bfloat16)
    grad_up = jnp.einsum(
        "rd,rf->df", saved_rows, up_grad, preferred_element_type=jnp.float32
    ).astype(jnp.bfloat16)
    partial_value = jnp.einsum(
        "rf,df->rd", gate_grad, gate_weight, preferred_element_type=jnp.float32
    )
    partial_value = partial_value + jnp.einsum(
        "rf,df->rd", up_grad, up_weight, preferred_element_type=jnp.float32
    )
    rounded_terms = partial_value.astype(jnp.bfloat16)
    reduced = (
        lax.psum_scatter(rounded_terms, "tp", scatter_dimension=1, tiled=True)
        .astype(jnp.float32)
        .astype(jnp.bfloat16)
    )
    returned = lax.all_to_all(
        reduced.reshape(sp_devices, capacity, -1), "sp", split_axis=0, concat_axis=0, tiled=True
    )
    returned = returned.reshape(sp_devices * capacity, -1)
    picked = returned[slot_index]
    picked = picked.reshape(tok_rows, top_count, -1)
    grad_routed = jnp.sum(picked.astype(jnp.float32), axis=1).astype(jnp.bfloat16)
    mixer_grad = jnp.einsum("td,cd->tc", full_grad, w_out, preferred_element_type=jnp.float32)
    mixed = (b_gate.astype(jnp.float32) * conv_out.astype(jnp.float32)).astype(jnp.bfloat16)
    projected = lax.psum_scatter(
        jnp.einsum("td,tc->dc", full_grad, mixed, preferred_element_type=jnp.float32),
        "sp",
        scatter_dimension=0,
        tiled=True,
    )
    grad_out_proj = projected.T
    out_grad = mixer_grad * b_gate.astype(jnp.float32)
    tap_reach = taps.shape[0] - 1
    following = passed_along(out_grad[:tap_reach], "sp", -1)
    extended = jnp.concatenate([out_grad, following], axis=0)
    tap_values = taps.astype(jnp.float32)
    conv_grad = jnp.zeros_like(out_grad)
    for tap_index in range(tap_reach + 1):
        offset = tap_reach - tap_index
        conv_grad = conv_grad + tap_values[tap_index] * extended[offset : offset + tok_rows]
    grad_conv_in = (conv_grad * c_gate.astype(jnp.float32)).astype(jnp.bfloat16)
    grad_c_gate = (conv_grad * conv_in.astype(jnp.float32)).astype(jnp.bfloat16)
    grad_b_gate = (mixer_grad * conv_out.astype(jnp.float32)).astype(jnp.bfloat16)
    return (
        grad_gate[None],
        grad_up[None],
        grad_down[None],
        grad_routed,
        grad_out_proj,
        grad_conv_in,
        grad_c_gate,
        grad_b_gate,
    )


def solution(mesh):
    in_specs = (
        P("sp", "tp"),
        P("sp", None),
        P("sp", None),
        P("sp", None, "tp"),
        P("sp", None, "tp"),
        P("sp", None, "tp"),
        P("sp", "tp", None),
        P("sp", "tp"),
        P("sp", "tp"),
        P("sp", "tp"),
        P("sp", "tp"),
        P(None, "tp"),
        P("tp", None),
    )
    out_specs = (
        P("sp", None, "tp"),
        P("sp", None, "tp"),
        P("sp", "tp", None),
        P("sp", "tp"),
        P("tp", "sp"),
        P("sp", "tp"),
        P("sp", "tp"),
        P("sp", "tp"),
    )
    return jax.shard_map(
        per_device, mesh=mesh, in_specs=in_specs, out_specs=out_specs, check_vma=False
    )
```

profile of v0, /device:TPU:0, one launch (start us, length us, event | category | flops | bytes accessed | tf_op | source)
XLA Modules:
  0.0 212.0 jit_solution(14027986862488300360)
XLA Ops:
  11.5 2.2 %mul.116 = f32[256,2,512]{2,1,0:T(2,128)} broadcast(bf16[256,512]{1,0:T(8,128)(2,1)} %param.13), dimensions={0,2} | broadcast | bytes 1310720 | tf_op jit(solution)/shard_map/mul | solution.py:43
  13.7 1.9 mul.117
  16.0 3.4 %scatter_custom_fusion = bf16[768,512]{1,0:T(8,128)(2,1)} fusion(s32[512]{0:T(512)S(1)} %bitcast.76, f32[512,512]{1,0:T(8,128)S(1)} %mul.117, f32[512]{0:T(512)S(1)} %mul.114, bf16[]{:T(256)} %constant.11.clone.1), kind=kCustom, calls=%fused_computation.36 | custom fusion | flops 524288 | bytes 1837058 | tf_op jit(solution)/shard_map/scatter | solution.py:46
  19.4 27.5 %all_to_all.10 = bf16[8,96,512]{2,1,0:T(8,128)(2,1)} all-to-all(bf16[8,96,512]{2,1,0:T(8,128)(2,1)} %bitcast.73), channel_id=1, replica_groups=mesh['sp'=8,'tp'=4] {'sp'}, dimensions={0} | all-to-all | bytes 1572864 | tf_op jit(solution)/shard_map/all_to_all | solution.py:48
  48.0 5.6 %fusion.4 = f32[768,512]{1,0:T(8,128)} fusion(bf16[1,768,2048]{2,1,0:T(8,128)(2,1)} %all-gather.9.cloned.1.call-done, bf16[1,2048,512]{2,1,0:T(8,128)(2,1)} %param.18), kind=kOutput, calls=%fused_computation.7 | convolution fusion | flops 1610612736 | bytes 6815744 | tf_op jit(solution)/shard_map/dot_general | solution.py:59
  53.6 3.0 %fusion.6 = f32[768,512]{1,0:T(8,128)} fusion(bf16[1,768,2048]{2,1,0:T(8,128)(2,1)S(1)} %copy-done.1, bf16[1,2048,512]{2,1,0:T(8,128)(2,1)S(1)} %copy-done), kind=kOutput, calls=%fused_computation.9 | convolution fusion | flops 1610612736 | bytes 6815744 | tf_op jit(solution)/shard_map/dot_general | solution.py:58
  56.6 18.1 %all-gather.5.cloned.1.call-done = bf16[768,2048]{1,0:T(8,128)(2,1)} async-done(((bf16[768,512]{1,0:T(8,128)(2,1)}), bf16[768,2048]{1,0:T(8,128)(2,1)}) %all-gather.5.cloned.1.call-update) | async-done | bytes 3145744 | tf_op jit(solution)/shard_map/all_gather | solution.py:52
  74.7 6.1 %select_convert_fusion = (bf16[768,512]{1,0:T(8,128)(2,1)S(1)}, bf16[768,512]{1,0:T(8,128)(2,1)S(1)}) fusion(f32[768,512]{1,0:T(8,128)} %fusion.4, f32[768,512]{1,0:T(8,128)} %fusion.6, bf16[768,2048]{1,0:T(8,128)(2,1)} %all-gather.5.cloned.1.call-done, bf16[1,512,2048]{2,1,0:T(8,128)(2,1)} %param.19), kind=kOutput, calls=%fused_computation.26 | convolution fusion | flops 1619263488 | bytes 9961472 | tf_op jit(solution)/shard_map/rd,fd->rf/dot_general | solution.py:64
  80.8 1.8 fusion.25
  83.0 3.5 %add_convert_fusion = bf16[768,2048]{1,0:T(8,128)(2,1)} fusion(f32[768,2048]{1,0:T(8,128)S(1)} %fusion.25, bf16[768,512]{1,0:T(8,128)(2,1)S(1)} %get-tuple-element.26, bf16[1,2048,512]{2,1,0:T(8,128)(2,1)S(1)} %copy-done.5), kind=kOutput, calls=%fused_computation.2 | convolution fusion | flops 1613758464 | bytes 12320768 | tf_op jit(solution)/shard_map/rf,df->rd/dot_general | solution.py:84
  87.3 5.7 %all-gather.7.cloned.1.call-done = bf16[256,2048]{1,0:T(8,128)(2,1)} async-done(((bf16[256,512]{1,0:T(8,128)(2,1)}), bf16[256,2048]{1,0:T(8,128)(2,1)}) %all-gather.7.cloned.1.call-update) | async-done | bytes 1048592 | tf_op jit(solution)/shard_map/all_gather | solution.py:35
  93.0 2.4 %fusion.40 = (bf16[256,128]{1,0:T(8,128)(2,1)}, f32[256,128]{1,0:T(8,128)S(1)}) fusion(bf16[256,128]{1,0:T(8,128)(2,1)S(1)} %copy-done.7, bf16[256,128]{1,0:T(8,128)(2,1)S(1)} %copy-done.8, bf16[256,2048]{1,0:T(8,128)(2,1)} %all-gather.7.cloned.1.call-done, bf16[128,2048]{1,0:T(8,128)(2,1)S(1)} %copy-done.6), kind=kOutput, calls=%fused_computation.49 | convolution fusion | flops 134381568 | bytes 1900544 | tf_op jit(solution)/shard_map/td,cd->tc/dot_general | solution.py:100
  95.4 1.4 collective-permute-start
  98.2 2.7 %collective-permute-done = f32[2,128]{1,0:T(2,128)S(1)} collective-permute-done((f32[2,128]{1,0:T(2,128)S(1)}, f32[2,128]{1,0:T(2,128)S(1)}, u32[]{:S(2)}, u32[]{:S(2)}) %collective-permute-start) | collective-permute-done | bytes 1056 | tf_op jit(solution)/shard_map/ppermute | solution.py:13
  102.3 30.8 %reduce-scatter.3.cloned.1.call-done = bf16[768,512]{1,0:T(8,128)(2,1)} async-done(((bf16[768,2048]{1,0:T(8,128)(2,1)}), bf16[768,512]{1,0:T(8,128)(2,1)}) %reduce-scatter.3.cloned.1.call-update) | async-done | bytes 786448 | tf_op jit(solution)/shard_map/reduce_scatter | solution.py:89
  133.1 5.5 %all-to-all-start.1 = ((bf16[8,96,512]{2,1,0:T(8,128)(2,1)}), bf16[8,96,512]{2,1,0:T(8,128)(2,1)S(1)}, u32[]{:S(2)}, u32[]{:S(2)}) async-start(bf16[8,96,512]{2,1,0:T(8,128)(2,1)} %bitcast.75), calls=%async_computation.2 | async-start | bytes 1572864 | tf_op jit(solution)/shard_map/all_to_all | solution.py:93
  138.6 5.3 %fusion.18 = bf16[1,2048,512]{1,2,0:T(8,128)(2,1)} fusion(bf16[768,512]{1,0:T(8,128)(2,1)} %copy-done.4, bf16[1,768,2048]{2,1,0:T(8,128)(2,1)} %all-gather.9.cloned.1.call-done), kind=kOutput, calls=%fused_computation.16 | convolution fusion | flops 1611661312 | bytes 6029312 | tf_op jit(solution)/shard_map/rd,rf->df/dot_general | solution.py:75
  143.9 3.9 %copy.27 = bf16[1,2048,512]{2,1,0:T(8,128)(2,1)} copy(bf16[1,2048,512]{1,2,0:T(8,128)(2,1)} %fusion.18) | data formatting | bytes 4194304
  147.8 5.3 %fusion.15 = bf16[1,2048,512]{1,2,0:T(8,128)(2,1)} fusion(bf16[768,512]{1,0:T(8,128)(2,1)} %copy-done.3, bf16[1,768,2048]{2,1,0:T(8,128)(2,1)} %all-gather.9.cloned.1.call-done), kind=kOutput, calls=%fused_computation.15 | convolution fusion | flops 1611661312 | bytes 6029312 | tf_op jit(solution)/shard_map/rd,rf->df/dot_general | solution.py:78
  153.1 3.9 %copy.28 = bf16[1,2048,512]{2,1,0:T(8,128)(2,1)} copy(bf16[1,2048,512]{1,2,0:T(8,128)(2,1)} %fusion.15) | data formatting | bytes 4194304
  157.0 6.2 %fusion.14 = bf16[1,512,2048]{2,1,0:T(8,128)(2,1)} fusion(bf16[768,2048]{1,0:T(8,128)(2,1)} %all-gather.5.cloned.1.call-done, f32[768,512]{1,0:T(8,128)} %fusion.6, f32[768,512]{1,0:T(8,128)} %fusion.4), kind=kOutput, calls=%fused_computation.14 | convolution fusion | flops 1615593472 | bytes 8388608 | tf_op jit(solution)/shard_map/rf,rd->fd/dot_general | solution.py:65
  164.6 2.0 gather_fusion
  166.7 2.1 reduce_sum.25
  168.8 36.7 %reduce-scatter.5.cloned.1.call-done = f32[256,128]{0,1:T(8,128)} async-done(((f32[2048,128]{0,1:T(8,128)}), f32[256,128]{0,1:T(8,128)}) %reduce-scatter.5.cloned.1.call-update) | async-done | bytes 131088 | tf_op jit(solution)/shard_map/reduce_scatter | solution.py:102
  (61 shorter events, 11.0 us)
Async XLA Ops:
  7.2 46.4 %copy-start = (bf16[1,2048,512]{2,1,0:T(8,128)(2,1)S(1)}, bf16[1,2048,512]{2,1,0:T(8,128)(2,1)}, u32[]{:S(2)}) copy-start(bf16[1,2048,512]{2,1,0:T(8,128)(2,1)} %param.17) | copy-start | bytes 6291460
  7.2 40.8 %all-gather.9.cloned.1.call-start = ((), (), s32[]{:S(2)}) async-start(), calls=%async_computation.8 | async-start | bytes 3932160 | tf_op jit(solution)/shard_map/all_gather | solution.py:53
  7.9 7.7 %copy-start.11 = (f32[256,2]{0,1:T(2,128)S(1)}, f32[256,2]{0,1:T(2,128)}, u32[]{:S(2)}) copy-start(f32[256,2]{0,1:T(2,128)} %param.15) | copy-start | bytes 6148
  7.9 66.7 %all-gather.5.cloned.1.call-start = ((), (), s32[]{:S(2)}) async-start(), calls=%async_computation.4 | async-start | bytes 3932160 | tf_op jit(solution)/shard_map/all_gather | solution.py:52
  47.0 46.0 %all-gather.7.cloned.1.call-start = ((), (), s32[]{:S(2)}) async-start(), calls=%async_computation.6 | async-start | bytes 1310720 | tf_op jit(solution)/shard_map/all_gather | solution.py:35
  47.7 85.4 %reduce-scatter.3.cloned.1.call-start = ((), (), s32[]{:S(2)}) async-start(), calls=%async_computation.5 | async-start | bytes 3932160 | tf_op jit(solution)/shard_map/reduce_scatter | solution.py:89
  47.9 5.6 %copy-start.1 = (bf16[1,768,2048]{2,1,0:T(8,128)(2,1)S(1)}, bf16[1,768,2048]{2,1,0:T(8,128)(2,1)}, u32[]{:S(2)}) copy-start(bf16[1,768,2048]{2,1,0:T(8,128)(2,1)} %all-gather.9.cloned.1.call-done) | copy-start | bytes 9437188
  80.8 1.9 copy-start.4
  80.8 1.9 copy-start.3
  80.8 2.2 %copy-start.5 = (bf16[1,2048,512]{2,1,0:T(8,128)(2,1)S(1)}, bf16[1,2048,512]{2,1,0:T(8,128)(2,1)}, u32[]{:S(2)}) copy-start(bf16[1,2048,512]{2,1,0:T(8,128)(2,1)} %param.18) | copy-start | bytes 6291460
  86.6 0.7 copy-start.12
  86.6 6.4 %copy-start.6 = (bf16[128,2048]{1,0:T(8,128)(2,1)S(1)}, bf16[128,2048]{1,0:T(8,128)(2,1)}, u32[]{:S(2)}) copy-start(bf16[128,2048]{1,0:T(8,128)(2,1)} %param.25) | copy-start | bytes 1572868
  86.6 6.4 %copy-start.7 = (bf16[256,128]{1,0:T(8,128)(2,1)S(1)}, bf16[256,128]{1,0:T(8,128)(2,1)}, u32[]{:S(2)}) copy-start(bf16[256,128]{1,0:T(8,128)(2,1)} %param.23) | copy-start | bytes 196612
  86.6 6.4 %copy-start.8 = (bf16[256,128]{1,0:T(8,128)(2,1)S(1)}, bf16[256,128]{1,0:T(8,128)(2,1)}, u32[]{:S(2)}) copy-start(bf16[256,128]{1,0:T(8,128)(2,1)} %param.22) | copy-start | bytes 196612
  86.6 118.9 %reduce-scatter.5.cloned.1.call-start = ((), (), s32[]{:S(2)}) async-start(), calls=%async_computation.7 | async-start | bytes 1179648 | tf_op jit(solution)/shard_map/reduce_scatter | solution.py:102
  93.0 3.8 %copy-start.2 = (bf16[256,2048]{1,0:T(8,128)(2,1)S(1)}, bf16[256,2048]{1,0:T(8,128)(2,1)}, u32[]{:S(2)}) copy-start(bf16[256,2048]{1,0:T(8,128)(2,1)} %all-gather.7.cloned.1.call-done) | copy-start | bytes 3145732
  95.4 5.6 %copy-start.9 = (bf16[256,128]{1,0:T(8,128)(2,1)S(1)}, bf16[256,128]{1,0:T(8,128)(2,1)}, u32[]{:S(2)}) copy-start(bf16[256,128]{1,0:T(8,128)(2,1)} %param.20) | copy-start | bytes 196612
  95.4 6.3 %copy-start.10 = (bf16[256,128]{1,0:T(8,128)(2,1)S(1)}, bf16[256,128]{1,0:T(8,128)(2,1)}, u32[]{:S(2)}) copy-start(bf16[256,128]{1,0:T(8,128)(2,1)} %param.21) | copy-start | bytes 196612
  95.4 5.6 %collective-permute-start = (f32[2,128]{1,0:T(2,128)S(1)}, f32[2,128]{1,0:T(2,128)S(1)}, u32[]{:S(2)}, u32[]{:S(2)}) collective-permute-start(f32[2,128]{1,0:T(2,128)S(1)} %slice.35), channel_id=1, source_target_pairs={{4,0},{8,4},{12,8},{16,12},{20,16},{24,20},{28,24},{5,1},{9,5},{13... | collective-permute-start | bytes 3080 | tf_op jit(solution)/shard_map/ppermute | solution.py:13
  133.1 31.5 %all-to-all-start.1 = ((bf16[8,96,512]{2,1,0:T(8,128)(2,1)}), bf16[8,96,512]{2,1,0:T(8,128)(2,1)S(1)}, u32[]{:S(2)}, u32[]{:S(2)}) async-start(bf16[8,96,512]{2,1,0:T(8,128)(2,1)} %bitcast.75), calls=%async_computation.2 | async-start | bytes 1572864 | tf_op jit(solution)/shard_map/all_to_all | solution.py:93
Sparse Core Ops, SparseCore 0:
  9.6 31.2 all-gather.8
  47.1 27.5 all-gather.4
  76.2 16.6 all-gather.6
  95.3 37.7 reduce-scatter.2
  136.9 68.5 reduce-scatter.4
where the time goes:
time: 213 us; the launch traced here: 212 us
  waiting for transfers between devices  96.8 us (45%)
  matrix products  40.6 us (19%)
  blocking collectives  27.5 us (13%)
  local copies, waits for them, and re-layouts  17 us (8%)
  between operations  14 us (7%)
  other arithmetic  8.79 us (4%)
  starting transfers between devices  7.3 us (3%)
    reduce_scatter x1, waiting for transfers between devices, per_device(): lax.psum_scatter(jnp.einsum('td,tc->dc', full_grad, mixed, preferred_elem...  36.7 us
    reduce_scatter x1, waiting for transfers between devices, per_device(): lax.psum_scatter(rounded_terms, 'tp', scatter_dimension=1, tiled=True)  30.8 us
    all_to_all x1, blocking collectives, per_device(): lax.all_to_all(buffer.reshape(sp_devices, capacity, -1), 'sp', split_axis...  27.5 us
    all_gather x1, waiting for transfers between devices, per_device(): lax.all_gather(arrived.reshape(sp_devices * capacity, -1), 'tp', axis=1,...  18.1 us
    unnamed x30, local copies, waits for them, and re-layouts  9.79 us
    dot_general x1, matrix products, per_device(): jnp.einsum('rf,rd->fd', hidden, expert_grad, preferred_element_type=jnp.f...  6.18 us
    dot_general x1, matrix products, per_device(): jnp.einsum('rd,fd->rf', expert_grad, down_weight, preferred_element_type=...  6.15 us
    all_gather x1, waiting for transfers between devices, per_device(): full_grad = lax.all_gather(layer_grad, 'tp', axis=1, tiled=True)  5.69 us
  transfers between devices with their start and end apart: 7, of which 6 were waited for; matrix products, arithmetic and copies ran while one was open for 31% of the time, Pallas kernels for 0%

commit v1 on v0

--- a/solution.py
+++ b/solution.py
@@ -5,6 +5,11 @@
 
 clamp_limit = 7.0
 swish_alpha = 1.702
+
+
+def all_parts(x, axis, d):
+    blocks = lax.all_gather(x, axis)
+    return jnp.concatenate(blocks, axis=d)
 
 
 def passed_along(value, axis, steps):
@@ -49,7 +54,7 @@
         buffer.reshape(sp_devices, capacity, -1), "sp", split_axis=0, concat_axis=0, tiled=True
     )
     expert_grad, saved_rows = (
-        lax.all_gather(arrived.reshape(sp_devices * capacity, -1), "tp", axis=1, tiled=True),
+        all_parts(arrived.reshape(sp_devices * capacity, -1), "tp", 1),
         lax.all_gather(expert_in[0], "tp", axis=1, tiled=True),
     )
     gate_weight = w_gate[0]

time: 213 us -> 213 us (level)
  waiting for transfers between devices: 96.8 us -> 91.8 us
  local copies, waits for them, and re-layouts: 17 us -> 21.6 us
    all_gather x1, waiting for transfers between devices: 5.69 us -> 0.98 us  [per_device(): full_grad = lax.all_gather(layer_grad, 'tp', axis=1, tiled=True)]
    all_gather x0 -> x1, local copies, waits for them, and re-layouts: none -> 4.66 us  [all_parts(): blocks = lax.all_gather(x, axis)]
  transfers between devices with their start and end apart: 7 -> 7, of which waited for: 6 -> 6; matrix products, arithmetic and copies ran while one was open for 31% -> 33% of each run, Pallas kernels for 0% -> 0%
where the time goes in v1:
time: 213 us; the launch traced here: 212 us
  waiting for transfers between devices  91.8 us (43%)
  matrix products  41 us (19%)
  blocking collectives  27.5 us (13%)
  local copies, waits for them, and re-layouts  21.6 us (10%)
  between operations  14 us (7%)
  other arithmetic  8.79 us (4%)
  starting transfers between devices  7.3 us (3%)
    reduce_scatter x1, waiting for transfers between devices, per_device(): lax.psum_scatter(jnp.einsum('td,tc->dc', full_grad, mixed, preferred_elem...  36.6 us
    reduce_scatter x1, waiting for transfers between devices, per_device(): lax.psum_scatter(rounded_terms, 'tp', scatter_dimension=1, tiled=True)  30.8 us
    all_to_all x1, blocking collectives, per_device(): lax.all_to_all(buffer.reshape(sp_devices, capacity, -1), 'sp', split_axis...  27.5 us
    all_gather x1, waiting for transfers between devices, all_parts(): blocks = lax.all_gather(x, axis)  18.1 us
    unnamed x30, local copies, waits for them, and re-layouts  9.74 us
    dot_general x1, matrix products, per_device(): jnp.einsum('rf,rd->fd', hidden, expert_grad, preferred_element_type=jnp.f...  6.41 us
    dot_general x1, matrix products, per_device(): jnp.einsum('rd,fd->rf', expert_grad, down_weight, preferred_element_type=...  6.25 us
    dot_general x1, matrix products, per_device(): up_pre = jnp.dot(saved_rows, up_weight, preferred_element_type=jnp.float32)  5.62 us
  transfers between devices with their start and end apart: 7, of which 6 were waited for; matrix products, arithmetic and copies ran while one was open for 33% of the time, Pallas kernels for 0%

profile of v1, /device:TPU:0, one launch (start us, length us, event | category | flops | bytes accessed | tf_op | source)
XLA Modules:
  0.0 212.0 jit_solution(17854373211226834599)
XLA Ops:
  11.5 2.2 %mul.116 = f32[256,2,512]{2,1,0:T(2,128)} broadcast(bf16[256,512]{1,0:T(8,128)(2,1)} %param.13), dimensions={0,2} | broadcast | bytes 1310720 | tf_op jit(solution)/shard_map/mul | solution.py:48
  13.7 1.9 mul.117
  16.0 3.4 %scatter_custom_fusion = bf16[768,512]{1,0:T(8,128)(2,1)} fusion(s32[512]{0:T(512)S(1)} %bitcast.81, f32[512,512]{1,0:T(8,128)S(1)} %mul.117, f32[512]{0:T(512)S(1)} %mul.114, bf16[]{:T(256)} %constant.11.clone.1), kind=kCustom, calls=%fused_computation.36 | custom fusion | flops 524288 | bytes 1837058 | tf_op jit(solution)/shard_map/scatter | solution.py:51
  19.4 27.5 %all_to_all.10 = bf16[8,96,512]{2,1,0:T(8,128)(2,1)} all-to-all(bf16[8,96,512]{2,1,0:T(8,128)(2,1)} %bitcast.76), channel_id=1, replica_groups=mesh['sp'=8,'tp'=4] {'sp'}, dimensions={0} | all-to-all | bytes 1572864 | tf_op jit(solution)/shard_map/all_to_all | solution.py:53
  48.0 5.6 %fusion.4 = f32[768,512]{1,0:T(8,128)} fusion(bf16[1,768,2048]{2,1,0:T(8,128)(2,1)} %all-gather.9.cloned.1.call-done, bf16[1,2048,512]{2,1,0:T(8,128)(2,1)} %param.18), kind=kOutput, calls=%fused_computation.7 | convolution fusion | flops 1610612736 | bytes 6815744 | tf_op jit(solution)/shard_map/dot_general | solution.py:64
  53.6 3.0 %fusion.6 = f32[768,512]{1,0:T(8,128)} fusion(bf16[1,768,2048]{2,1,0:T(8,128)(2,1)S(1)} %copy-done.1, bf16[1,2048,512]{2,1,0:T(8,128)(2,1)S(1)} %copy-done), kind=kOutput, calls=%fused_computation.9 | convolution fusion | flops 1610612736 | bytes 6815744 | tf_op jit(solution)/shard_map/dot_general | solution.py:63
  56.6 18.1 %all-gather.5.cloned.1.call-done = bf16[4,768,512]{2,1,0:T(8,128)(2,1)} async-done(((bf16[1,768,512]{2,1,0:T(8,128)(2,1)}), bf16[4,768,512]{2,1,0:T(8,128)(2,1)}) %all-gather.5.cloned.1.call-update) | async-done | bytes 3145744 | tf_op jit(solution)/shard_map/all_gather | solution.py:11
  74.7 4.7 %copy.41 = bf16[4,768,512]{1,2,0:T(8,128)(2,1)} copy(bf16[4,768,512]{2,1,0:T(8,128)(2,1)} %all-gather.5.cloned.1.call-done) | data formatting | bytes 6291456 | tf_op jit(solution)/shard_map/all_gather | solution.py:11
  79.3 6.2 %select_convert_fusion = (bf16[768,512]{1,0:T(8,128)(2,1)S(1)}, bf16[768,512]{1,0:T(8,128)(2,1)S(1)}) fusion(f32[768,512]{1,0:T(8,128)} %fusion.4, f32[768,512]{1,0:T(8,128)} %fusion.6, bf16[768,2048]{0,1:T(8,128)(2,1)} %bitcast.77, bf16[1,512,2048]{2,1,0:T(8,128)(2,1)} %param.19), kind=kOutput, calls=%fused_computation.26 | convolution fusion | flops 1619263488 | bytes 9961472 | tf_op jit(solution)/shard_map/rd,fd->rf/dot_general | solution.py:69
  85.6 1.8 fusion.25
  87.8 3.5 %add_convert_fusion = bf16[768,2048]{1,0:T(8,128)(2,1)} fusion(f32[768,2048]{1,0:T(8,128)S(1)} %fusion.25, bf16[768,512]{1,0:T(8,128)(2,1)S(1)} %get-tuple-element.42, bf16[1,2048,512]{2,1,0:T(8,128)(2,1)S(1)} %copy-done.5), kind=kOutput, calls=%fused_computation.2 | convolution fusion | flops 1613758464 | bytes 12320768 | tf_op jit(solution)/shard_map/rf,df->rd/dot_general | solution.py:89
  93.0 2.4 %fusion.40 = (bf16[256,128]{1,0:T(8,128)(2,1)}, f32[256,128]{1,0:T(8,128)S(1)}) fusion(bf16[256,128]{1,0:T(8,128)(2,1)S(1)} %copy-done.7, bf16[256,128]{1,0:T(8,128)(2,1)S(1)} %copy-done.8, bf16[256,2048]{1,0:T(8,128)(2,1)} %all-gather.7.cloned.1.call-done, bf16[128,2048]{1,0:T(8,128)(2,1)S(1)} %copy-done.6), kind=kOutput, calls=%fused_computation.49 | convolution fusion | flops 134381568 | bytes 1900544 | tf_op jit(solution)/shard_map/td,cd->tc/dot_general | solution.py:105
  95.4 1.4 collective-permute-start
  98.2 2.7 %collective-permute-done = f32[2,128]{1,0:T(2,128)S(1)} collective-permute-done((f32[2,128]{1,0:T(2,128)S(1)}, f32[2,128]{1,0:T(2,128)S(1)}, u32[]{:S(2)}, u32[]{:S(2)}) %collective-permute-start) | collective-permute-done | bytes 1056 | tf_op jit(solution)/shard_map/ppermute | solution.py:18
  102.3 30.8 %reduce-scatter.3.cloned.1.call-done = bf16[768,512]{1,0:T(8,128)(2,1)} async-done(((bf16[768,2048]{1,0:T(8,128)(2,1)}), bf16[768,512]{1,0:T(8,128)(2,1)}) %reduce-scatter.3.cloned.1.call-update) | async-done | bytes 786448 | tf_op jit(solution)/shard_map/reduce_scatter | solution.py:94
  133.1 5.5 %all-to-all-start.1 = ((bf16[8,96,512]{2,1,0:T(8,128)(2,1)}), bf16[8,96,512]{2,1,0:T(8,128)(2,1)S(1)}, u32[]{:S(2)}, u32[]{:S(2)}) async-start(bf16[8,96,512]{2,1,0:T(8,128)(2,1)} %bitcast.80), calls=%async_computation.2 | async-start | bytes 1572864 | tf_op jit(solution)/shard_map/all_to_all | solution.py:98
  138.6 5.3 %fusion.18 = bf16[1,2048,512]{1,2,0:T(8,128)(2,1)} fusion(bf16[768,512]{1,0:T(8,128)(2,1)} %copy-done.4, bf16[1,768,2048]{2,1,0:T(8,128)(2,1)} %all-gather.9.cloned.1.call-done), kind=kOutput, calls=%fused_computation.16 | convolution fusion | flops 1611661312 | bytes 6029312 | tf_op jit(solution)/shard_map/rd,rf->df/dot_general | solution.py:80
  143.9 3.9 %copy.42 = bf16[1,2048,512]{2,1,0:T(8,128)(2,1)} copy(bf16[1,2048,512]{1,2,0:T(8,128)(2,1)} %fusion.18) | data formatting | bytes 4194304
  147.8 5.3 %fusion.15 = bf16[1,2048,512]{1,2,0:T(8,128)(2,1)} fusion(bf16[768,512]{1,0:T(8,128)(2,1)} %copy-done.3, bf16[1,768,2048]{2,1,0:T(8,128)(2,1)} %all-gather.9.cloned.1.call-done), kind=kOutput, calls=%fused_computation.15 | convolution fusion | flops 1611661312 | bytes 6029312 | tf_op jit(solution)/shard_map/rd,rf->df/dot_general | solution.py:83
  153.1 3.9 %copy.43 = bf16[1,2048,512]{2,1,0:T(8,128)(2,1)} copy(bf16[1,2048,512]{1,2,0:T(8,128)(2,1)} %fusion.15) | data formatting | bytes 4194304
  157.0 6.4 %fusion.14 = bf16[1,512,2048]{2,1,0:T(8,128)(2,1)} fusion(bf16[768,2048]{0,1:T(8,128)(2,1)} %bitcast.78, f32[768,512]{1,0:T(8,128)} %fusion.6, f32[768,512]{1,0:T(8,128)} %fusion.4), kind=kOutput, calls=%fused_computation.14 | convolution fusion | flops 1615593472 | bytes 8388608 | tf_op jit(solution)/shard_map/rf,rd->fd/dot_general | solution.py:70
  164.6 2.0 gather_fusion
  166.7 2.1 reduce_sum.25
  168.8 36.6 %reduce-scatter.5.cloned.1.call-done = f32[256,128]{0,1:T(8,128)} async-done(((f32[2048,128]{0,1:T(8,128)}), f32[256,128]{0,1:T(8,128)}) %reduce-scatter.5.cloned.1.call-update) | async-done | bytes 131088 | tf_op jit(solution)/shard_map/reduce_scatter | solution.py:107
  (62 shorter events, 11.6 us)
Async XLA Ops:
  7.2 46.4 %copy-start = (bf16[1,2048,512]{2,1,0:T(8,128)(2,1)S(1)}, bf16[1,2048,512]{2,1,0:T(8,128)(2,1)}, u32[]{:S(2)}) copy-start(bf16[1,2048,512]{2,1,0:T(8,128)(2,1)} %param.17) | copy-start | bytes 6291460
  7.2 40.8 %all-gather.9.cloned.1.call-start = ((), (), s32[]{:S(2)}) async-start(), calls=%async_computation.8 | async-start | bytes 3932160 | tf_op jit(solution)/shard_map/all_gather | solution.py:58
  7.9 7.7 %copy-start.11 = (f32[256,2]{0,1:T(2,128)S(1)}, f32[256,2]{0,1:T(2,128)}, u32[]{:S(2)}) copy-start(f32[256,2]{0,1:T(2,128)} %param.15) | copy-start | bytes 6148
  7.9 66.7 %all-gather.5.cloned.1.call-start = ((), (), s32[]{:S(2)}) async-start(), calls=%async_computation.4 | async-start | bytes 3932160 | tf_op jit(solution)/shard_map/all_gather | solution.py:11
  47.0 46.0 %all-gather.7.cloned.1.call-start = ((), (), s32[]{:S(2)}) async-start(), calls=%async_computation.6 | async-start | bytes 1310720 | tf_op jit(solution)/shard_map/all_gather | solution.py:40
  47.7 85.4 %reduce-scatter.3.cloned.1.call-start = ((), (), s32[]{:S(2)}) async-start(), calls=%async_computation.5 | async-start | bytes 3932160 | tf_op jit(solution)/shard_map/reduce_scatter | solution.py:94
  47.9 5.6 %copy-start.1 = (bf16[1,768,2048]{2,1,0:T(8,128)(2,1)S(1)}, bf16[1,768,2048]{2,1,0:T(8,128)(2,1)}, u32[]{:S(2)}) copy-start(bf16[1,768,2048]{2,1,0:T(8,128)(2,1)} %all-gather.9.cloned.1.call-done) | copy-start | bytes 9437188
  85.6 1.9 copy-start.4
  85.6 1.9 copy-start.3
  85.6 2.2 %copy-start.5 = (bf16[1,2048,512]{2,1,0:T(8,128)(2,1)S(1)}, bf16[1,2048,512]{2,1,0:T(8,128)(2,1)}, u32[]{:S(2)}) copy-start(bf16[1,2048,512]{2,1,0:T(8,128)(2,1)} %param.18) | copy-start | bytes 6291460
  91.3 0.7 copy-start.12
  91.3 1.7 copy-start.6
  91.3 1.7 copy-start.7
  91.3 1.7 copy-start.8
  91.3 114.1 %reduce-scatter.5.cloned.1.call-start = ((), (), s32[]{:S(2)}) async-start(), calls=%async_computation.7 | async-start | bytes 1179648 | tf_op jit(solution)/shard_map/reduce_scatter | solution.py:107
  93.0 3.8 %copy-start.2 = (bf16[256,2048]{1,0:T(8,128)(2,1)S(1)}, bf16[256,2048]{1,0:T(8,128)(2,1)}, u32[]{:S(2)}) copy-start(bf16[256,2048]{1,0:T(8,128)(2,1)} %all-gather.7.cloned.1.call-done) | copy-start | bytes 3145732
  95.4 5.6 %copy-start.9 = (bf16[256,128]{1,0:T(8,128)(2,1)S(1)}, bf16[256,128]{1,0:T(8,128)(2,1)}, u32[]{:S(2)}) copy-start(bf16[256,128]{1,0:T(8,128)(2,1)} %param.20) | copy-start | bytes 196612
  95.4 6.3 %copy-start.10 = (bf16[256,128]{1,0:T(8,128)(2,1)S(1)}, bf16[256,128]{1,0:T(8,128)(2,1)}, u32[]{:S(2)}) copy-start(bf16[256,128]{1,0:T(8,128)(2,1)} %param.21) | copy-start | bytes 196612
  95.4 5.6 %collective-permute-start = (f32[2,128]{1,0:T(2,128)S(1)}, f32[2,128]{1,0:T(2,128)S(1)}, u32[]{:S(2)}, u32[]{:S(2)}) collective-permute-start(f32[2,128]{1,0:T(2,128)S(1)} %slice.35), channel_id=1, source_target_pairs={{4,0},{8,4},{12,8},{16,12},{20,16},{24,20},{28,24},{5,1},{9,5},{13... | collective-permute-start | bytes 3080 | tf_op jit(solution)/shard_map/ppermute | solution.py:18
  133.1 31.5 %all-to-all-start.1 = ((bf16[8,96,512]{2,1,0:T(8,128)(2,1)}), bf16[8,96,512]{2,1,0:T(8,128)(2,1)S(1)}, u32[]{:S(2)}, u32[]{:S(2)}) async-start(bf16[8,96,512]{2,1,0:T(8,128)(2,1)} %bitcast.80), calls=%async_computation.2 | async-start | bytes 1572864 | tf_op jit(solution)/shard_map/all_to_all | solution.py:98
Sparse Core Ops, SparseCore 0:
  9.6 31.2 all-gather.8
  47.1 27.5 all-gather.4
  76.2 16.6 all-gather.6
  95.3 37.7 reduce-scatter.2
  136.9 68.4 reduce-scatter.4
